TPU v7x, 32 devices: a whole 2x2x4 slice. The times are simulated.
32 devices in a mesh: ep: 8 (over z, x), tp: 4 (over y, core).
Axes of the slice: x: 2, y: 2, z: 4, core: 2. Of those that a mesh axis runs over, the one named last changes fastest.
Arguments:
- mix_input: bfloat16 [1024, 2048], P('ep'), may hold values from -6 to 6
- mix_gain: float32 [2048], replicated, may hold values from 0.1 to 1.9
- pool_in_weight: bfloat16 [2048, 1024], P(None, 'tp'), may hold values from -0.125 to 0.125
- pool_out_weight: bfloat16 [1024, 2048], P(None, 'tp'), may hold values from -0.1875 to 0.1875
- moe_input: bfloat16 [1536, 2048], P('ep'), may hold values from -6 to 6
- moe_gain: float32 [2048], replicated, may hold values from 0.1 to 1.9
- group_router: bfloat16 [2048, 4], replicated, may hold values from -0.125 to 0.125
- expert_router: bfloat16 [2048, 8], replicated, may hold values from -0.125 to 0.125
- routes: int32 [1536, 2], P('ep'), may hold values from 0 to 7, as said below
- expert_gate: bfloat16 [8, 2048, 4096], P('ep', None, 'tp'), may hold values from -0.125 to 0.125
- expert_up: bfloat16 [8, 2048, 4096], P('ep', None, 'tp'), may hold values from -0.125 to 0.125
- expert_down: bfloat16 [8, 4096, 2048], P('ep', 'tp'), may hold values from -0.375 to 0.375
Outputs:
- mixed: bfloat16 [1024, 2048], P('ep', 'tp')
- experts_out: bfloat16 [1536, 2048], P('ep', 'tp')
Inputs may be any that keep to these rules, and one draw needn't show every extreme that they name: `routes`: each row names two different experts of one group: the 2 experts numbered k * 2 to k * 2 + 1 for a group k. Among the rows of one device no expert is named more than 96 times, and in the rows of every device some expert is named exactly 96 times.
All inputs are finite; a program needn't handle non-finite values.
Results may differ from a plain program's by a relative error of at most 0.019.
Values may be sent and summed in bfloat16 or wider, within the bound.
A program may use at most 64 MiB of HBM per device.

v0:
```python
import jax
import jax.numpy as jnp
from jax import lax
from jax.sharding import PartitionSpec as P

epsilon = 1e-06
pool_reach = 8


def with_halo(x, sides, width):
    for axis, dim in sides:
        devices, length = (lax.axis_size(axis), x.shape[dim])
        up = [(i, (i + 1) % devices) for i in range(devices - 1)]
        down = [(j, i) for i, j in up]
        last = lax.slice_in_dim(x, length - width, length, axis=dim)
        first = lax.slice_in_dim(x, 0, width, axis=dim)
        before = lax.ppermute(last, axis, up)
        after = lax.ppermute(first, axis, down)
        x = jnp.concatenate([before, x, after], axis=dim)
    return x


def normalize(row_data, gain_vector):
    values = row_data.astype(jnp.float32)
    inverse_rms = lax.rsqrt(jnp.mean(values * values, axis=-1, keepdims=True) + epsilon)
    return (values * inverse_rms * gain_vector).astype(jnp.bfloat16)


def pooled_block(pool_input):
    local_rows = pool_input.shape[0]
    part_channels = pool_input.shape[1]
    group_width = part_channels * lax.axis_size("tp") // 4
    group_index = lax.axis_index("tp") * part_channels // group_width
    half_span = jnp.left_shift(jnp.int32(1), group_index)
    extended = with_halo(pool_input, (("ep", 0),), pool_reach)
    totals = jnp.concatenate(
        [
            jnp.zeros((1, part_channels), jnp.float32),
            jnp.cumsum(extended.astype(jnp.float32), axis=0),
        ],
        axis=0,
    )
    upper_sum = lax.dynamic_slice_in_dim(totals, pool_reach + half_span, local_rows, 0)
    lower_sum = lax.dynamic_slice_in_dim(totals, pool_reach - half_span, local_rows, 0)
    places = lax.axis_index("ep") * local_rows + jnp.arange(local_rows, dtype=jnp.int32)
    length = local_rows * lax.axis_size("ep")
    counts = (jnp.minimum(places + half_span, length) - jnp.maximum(places - half_span, 0)).astype(
        jnp.float32
    )
    window_mean = (upper_sum - lower_sum) / counts[:, None]
    return (window_mean - pool_input.astype(jnp.float32)).astype(jnp.bfloat16)


def token_mixer(mix_input, mix_gain, pool_in_weight, pool_out_weight):
    normed = normalize(mix_input, mix_gain)
    pool_input = jnp.dot(normed, pool_in_weight, preferred_element_type=jnp.float32).astype(
        jnp.bfloat16
    )
    pooled = pooled_block(pool_input)
    projected = jnp.dot(
        lax.all_gather(pooled, "tp", axis=1, tiled=True),
        pool_out_weight,
        preferred_element_type=jnp.float32,
    )
    return projected.astype(jnp.bfloat16)


def routing(normed, group_router, expert_router, routes):
    group_logits = jnp.dot(normed, group_router, preferred_element_type=jnp.float32)
    expert_logits = jnp.dot(normed, expert_router, preferred_element_type=jnp.float32)
    group_count = group_router.shape[1]
    expert_count = expert_router.shape[1]
    per_group = expert_count // group_count
    first_id = routes[:, 0]
    second_id = routes[:, 1]
    chosen_group = first_id // per_group
    group_match = jnp.arange(group_count, dtype=jnp.int32)[None, :] == chosen_group[:, None]
    chosen_logit = jnp.sum(jnp.where(group_match, group_logits, 0.0), axis=1)
    group_share = 1.0 / jnp.sum(jnp.exp(group_logits - chosen_logit[:, None]), axis=1)
    expert_ids = jnp.arange(expert_count, dtype=jnp.int32)[None, :]
    first_logit = jnp.sum(jnp.where(expert_ids == first_id[:, None], expert_logits, 0.0), axis=1)
    second_logit = jnp.sum(jnp.where(expert_ids == second_id[:, None], expert_logits, 0.0), axis=1)
    first_weight = group_share * jax.nn.sigmoid(first_logit - second_logit)
    second_weight = group_share * jax.nn.sigmoid(second_logit - first_logit)
    return (first_weight, second_weight)


def routed_experts(
    moe_input, moe_gain, group_router, expert_router, routes, expert_gate, expert_up, expert_down
):
    normed = normalize(moe_input, moe_gain)
    first_weight, second_weight = routing(normed, group_router, expert_router, routes)
    local_rows = normed.shape[0]
    features = normed.shape[1]
    expert_count = expert_router.shape[1]
    capacity = 4 * local_rows // expert_count
    copies = 2 * local_rows
    copy_ids = routes.reshape(-1)
    onehot = (copy_ids[:, None] == jnp.arange(expert_count, dtype=jnp.int32)[None, :]).astype(
        jnp.int32
    )
    earlier = jnp.cumsum(onehot, axis=0) - onehot
    slot_rank = jnp.sum(earlier * onehot, axis=1)
    slot_index = copy_ids * capacity + slot_rank
    slot_copy = (
        jnp.full((expert_count * capacity,), copies, jnp.int32)
        .at[slot_index]
        .set(jnp.arange(copies, dtype=jnp.int32))
    )
    padded = jnp.concatenate([normed, jnp.zeros((1, features), jnp.bfloat16)], axis=0)
    outgoing = padded[slot_copy // 2].reshape(expert_count, capacity, features)
    part_width = features // lax.axis_size("tp")
    outgoing = lax.dynamic_slice_in_dim(outgoing, lax.axis_index("tp") * part_width, part_width, 2)
    arrived = lax.all_to_all(outgoing, "ep", split_axis=0, concat_axis=0, tiled=True)
    arrived = lax.all_gather(arrived, "tp", axis=2, tiled=True)
    sources = arrived.shape[0]
    item_count = arrived.shape[1]
    flat_rows = arrived.reshape(sources * item_count, features)
    gate_values = jnp.dot(flat_rows, expert_gate[0], preferred_element_type=jnp.float32)
    up_values = jnp.dot(flat_rows, expert_up[0], preferred_element_type=jnp.float32)
    hidden = (jax.nn.silu(gate_values) * up_values).astype(jnp.bfloat16)
    partial_out = jnp.dot(hidden, expert_down[0], preferred_element_type=jnp.float32)
    summed = lax.psum_scatter(
        partial_out.reshape(sources, item_count, features).astype(jnp.bfloat16),
        "tp",
        scatter_dimension=2,
        tiled=True,
    )
    returned = lax.all_to_all(summed, "ep", split_axis=0, concat_axis=0, tiled=True)
    flat_back = returned.reshape(expert_count * capacity, returned.shape[2])
    picked = flat_back[slot_index].astype(jnp.float32).reshape(local_rows, 2, returned.shape[2])
    combined = first_weight[:, None] * picked[:, 0] + second_weight[:, None] * picked[:, 1]
    return combined.astype(jnp.bfloat16)


def on_device(
    mix_input,
    mix_gain,
    pool_in_weight,
    pool_out_weight,
    moe_input,
    moe_gain,
    group_router,
    expert_router,
    routes,
    expert_gate,
    expert_up,
    expert_down,
):
    mixed = token_mixer(mix_input, mix_gain, pool_in_weight, pool_out_weight)
    experts_out = routed_experts(
        moe_input,
        moe_gain,
        group_router,
        expert_router,
        routes,
        expert_gate,
        expert_up,
        expert_down,
    )
    return (mixed, experts_out)


def solution(mesh):
    in_specs = (
        P("ep", None),
        P(),
        P(None, "tp"),
        P(None, "tp"),
        P("ep", None),
        P(),
        P(),
        P(),
        P("ep", None),
        P("ep", None, "tp"),
        P("ep", None, "tp"),
        P("ep", "tp", None),
    )
    out_specs = (P("ep", "tp"), P("ep", "tp"))
    return jax.shard_map(
        on_device, mesh=mesh, in_specs=in_specs, out_specs=out_specs, check_vma=False
    )
```

profile of v0, /device:TPU:0, one launch (start us, length us, event | category | flops | bytes accessed | tf_op | source)
XLA Modules:
  0.0 166.2 jit_solution(15513747708480736096)
XLA Ops:
  7.2 0.0 copy-start
  7.2 0.0 all-gather.2.cloned.1.call-start
  7.2 0.8 broadcast_multiply_fusion
  8.0 0.8 copy.21
  8.8 0.1 eq.86
  8.9 0.1 eq.82
  9.1 1.4 fusion.11
  10.5 0.1 copy.20
  10.6 0.1 mul.119
  10.8 0.9 reduce-window.16
  11.6 0.2 slice_reduce_fusion
  11.9 0.1 fusion.31
  12.0 2.9 %scatter_custom_fusion = s32[768]{0:T(1024)S(1)} fusion(s32[384]{0:T(512)S(1)} %fusion.37, s32[384]{0:T(512)S(1)} %iota.23, s32[]{:T(128)} %constant.91.clone.1), kind=kCustom, calls=%fused_computation.71 | custom fusion | bytes 3076 | tf_op jit(solution)/shard_map/scatter | solution.py:108
  15.0 1.4 fusion.13
  16.4 0.1 concatenate.11
  16.5 4.3 %gather_fusion = bf16[768,2048]{1,0:T(8,128)(2,1)} fusion(bf16[193,2048]{1,0:T(8,128)(2,1)S(1)} %concatenate.11, s32[1024]{0:T(1024)S(1)} %pad_clamp_fusion.1), kind=kCustom, calls=%fused_computation | custom fusion | bytes 6294528 | tf_op jit(solution)/shard_map/gather | solution.py:111
  20.7 1.2 constant_dynamic-slice_fusion
  21.9 27.3 %all_to_all.10 = bf16[8,96,512]{2,1,0:T(8,128)(2,1)} all-to-all(bf16[8,96,512]{2,1,0:T(8,128)(2,1)S(1)} %constant_dynamic-slice_fusion), channel_id=1, replica_groups=mesh['ep'=8,'tp'=4] {'ep'}, dimensions={0} | all-to-all | bytes 1572864 | tf_op jit(solution)/shard_map/all_to_all | solution.py:114
  49.2 0.0 all-gather.2.cloned.1.call-update
  49.3 0.0 reduce-scatter.2.cloned.1.call-start
  49.3 27.7 %all-gather.2.cloned.1.call-done = bf16[8,96,2048]{2,1,0:T(8,128)(2,1)} async-done(((bf16[8,96,512]{2,1,0:T(8,128)(2,1)}), bf16[8,96,2048]{2,1,0:T(8,128)(2,1)}) %all-gather.2.cloned.1.call-update) | async-done | bytes 3145744 | tf_op jit(solution)/shard_map/all_gather | solution.py:115
  77.0 6.3 %fusion.2 = f32[768,1024]{1,0:T(8,128)S(1)} fusion(bf16[768,2048]{1,0:T(8,128)(2,1)} %bitcast.78, bf16[1,2048,1024]{2,1,0:T(8,128)(2,1)} %param.22), kind=kOutput, calls=%fused_computation.5 | convolution fusion | flops 3221225472 | bytes 10485760 | tf_op jit(solution)/shard_map/dot_general | solution.py:120
  83.3 0.0 copy-start.6
  83.3 3.8 %multiply_convert_fusion = bf16[768,1024]{1,0:T(8,128)(2,1)S(1)} fusion(f32[768,1024]{1,0:T(8,128)S(1)} %fusion.2, bf16[768,2048]{1,0:T(8,128)(2,1)S(1)} %bitcast.79, bf16[1,2048,1024]{2,1,0:T(8,128)(2,1)S(1)} %copy-done.5), kind=kOutput, calls=%fused_computation.10 | convolution fusion | flops 3225944064 | bytes 12058624 | tf_op jit(solution)/shard_map/dot_general | solution.py:119
  87.1 4.8 %fusion.6 = bf16[8,96,2048]{2,1,0:T(8,128)(2,1)} fusion(bf16[8,96,1024]{2,1,0:T(8,128)(2,1)S(1)} %bitcast.80, bf16[1,1024,2048]{2,1,0:T(8,128)(2,1)S(1)} %copy-done.6), kind=kOutput, calls=%fused_computation.9 | convolution fusion | flops 3222798336 | bytes 8912896 | tf_op jit(solution)/shard_map/dot_general | solution.py:122
  91.9 0.0 copy-start.4
  91.9 0.0 copy-start.2
  91.9 0.0 reduce-scatter.2.cloned.1.call-update
  92.0 1.0 copy-done.1
  92.9 0.2 fusion.14
  93.1 0.2 copy-done.8
  93.3 0.4 convolution_convert_fusion.1
  93.7 3.4 %collective-permute-start = (bf16[8,256]{1,0:T(8,128)(2,1)S(1)}, bf16[8,256]{1,0:T(8,128)(2,1)S(1)}, u32[]{:S(2)}, u32[]{:S(2)}) collective-permute-start(bf16[8,256]{1,0:T(8,128)(2,1)S(1)} %get-tuple-element.6), channel_id=1, source_target_pairs={{0,4},{4,8},{8,12},{12,16},{16,20},{20,24},{24,28},{1,5},{5,9},{9,... | collective-permute-start | bytes 12296 | tf_op jit(solution)/shard_map/ppermute | solution.py:17
  97.0 1.3 collective-permute-start.1
  98.4 0.3 select_reduce_fusion.2
  98.8 0.3 select_reduce_fusion.1
  99.2 30.7 %reduce-scatter.2.cloned.1.call-done = bf16[8,96,512]{2,1,0:T(8,128)(2,1)} async-done(((bf16[8,96,2048]{2,1,0:T(8,128)(2,1)}), bf16[8,96,512]{2,1,0:T(8,128)(2,1)}) %reduce-scatter.2.cloned.1.call-update) | async-done | bytes 786448 | tf_op jit(solution)/shard_map/reduce_scatter | solution.py:123
  129.8 5.5 %all-to-all-start.1 = ((bf16[8,96,512]{2,1,0:T(8,128)(2,1)}), bf16[8,96,512]{2,1,0:T(8,128)(2,1)S(1)}, u32[]{:S(2)}, u32[]{:S(2)}) async-start(bf16[8,96,512]{2,1,0:T(8,128)(2,1)} %reduce-scatter.2.cloned.1.call-done), calls=%async_computation.2 | async-start | bytes 1572864 | tf_op jit(solution)/shard_map/all_to_all | solution.py:129
  135.3 0.0 collective-permute-done
  135.4 0.2 fusion.24
  135.8 0.1 fusion.29
  135.9 6.0 %all_gather.6 = bf16[128,1024]{1,0:T(8,128)(2,1)S(1)} all-gather(bf16[128,256]{1,0:T(8,128)(2,1)S(1)} %fusion.29), channel_id=1, replica_groups=mesh['ep'=8,'tp'=4] {'tp'}, dimensions={1}, use_global_device_ids=true | all-gather | bytes 327680 | tf_op jit(solution)/shard_map/all_gather | solution.py:61
  141.8 1.0 convolution_convert_fusion
  142.8 12.6 %all-to-all-done.1 = bf16[8,96,512]{2,1,0:T(8,128)(2,1)S(1)} async-done(((bf16[8,96,512]{2,1,0:T(8,128)(2,1)}), bf16[8,96,512]{2,1,0:T(8,128)(2,1)S(1)}, u32[]{:S(2)}, u32[]{:S(2)}) %all-to-all-start.1) | async-done | bytes 786464 | tf_op jit(solution)/shard_map/all_to_all | solution.py:129
  155.4 2.1 %gather_fusion.1 = bf16[384,512]{1,0:T(8,128)(2,1)S(1)} fusion(bf16[768,512]{1,0:T(8,128)(2,1)S(1)} %bitcast.67, s32[1024]{0:T(1024)S(1)} %pad_clamp_fusion), kind=kCustom, calls=%fused_computation.1 | custom fusion | bytes 787968 | tf_op jit(solution)/shard_map/gather | solution.py:131
  157.5 0.5 reshape.137
  158.0 0.6 fusion.38
  158.6 0.8 fusion.22
  (39 shorter events, 0.4 us)
Async XLA Ops:
  7.2 134.7 %copy-start = (bf16[1024,512]{1,0:T(8,128)(2,1)S(1)}, bf16[1024,512]{1,0:T(8,128)(2,1)}, u32[]{:S(2)}) copy-start(bf16[1024,512]{1,0:T(8,128)(2,1)} %param.15) | copy-start | bytes 3145732
  7.2 69.8 %all-gather.2.cloned.1.call-start = ((), (), s32[]{:S(2)}) async-start(), calls=%async_computation.3 | async-start | bytes 3932160 | tf_op jit(solution)/shard_map/all_gather | solution.py:115
  49.3 80.6 %reduce-scatter.2.cloned.1.call-start = ((), (), s32[]{:S(2)}) async-start(), calls=%async_computation.4 | async-start | bytes 3932160 | tf_op jit(solution)/shard_map/reduce_scatter | solution.py:123
  77.0 6.3 %copy-start.5 = (bf16[1,2048,1024]{2,1,0:T(8,128)(2,1)S(1)}, bf16[1,2048,1024]{2,1,0:T(8,128)(2,1)}, u32[]{:S(2)}) copy-start(bf16[1,2048,1024]{2,1,0:T(8,128)(2,1)} %param.21) | copy-start | bytes 12582916
  77.0 6.3 %copy-start.7 = (bf16[8,96,2048]{2,1,0:T(8,128)(2,1)S(1)}, bf16[8,96,2048]{2,1,0:T(8,128)(2,1)}, u32[]{:S(2)}) copy-start(bf16[8,96,2048]{2,1,0:T(8,128)(2,1)} %all-gather.2.cloned.1.call-done) | copy-start | bytes 9437188
  83.3 3.8 %copy-start.6 = (bf16[1,1024,2048]{2,1,0:T(8,128)(2,1)S(1)}, bf16[1,1024,2048]{2,1,0:T(8,128)(2,1)}, u32[]{:S(2)}) copy-start(bf16[1,1024,2048]{2,1,0:T(8,128)(2,1)} %param.23) | copy-start | bytes 12582916
  91.9 1.0 copy-start.1
  91.9 1.4 copy-start.8
  91.9 1.4 copy-start.9
  91.9 6.5 %copy-start.3 = (s32[192,2]{0,1:T(2,128)S(1)}, s32[192,2]{0,1:T(2,128)}, u32[]{:S(2)}) copy-start(s32[192,2]{0,1:T(2,128)} %param.20) | copy-start | bytes 4612
  91.9 6.5 %copy-start.4 = (bf16[2048,4]{0,1:T(4,128)(2,1)S(1)}, bf16[2048,4]{0,1:T(4,128)(2,1)}, u32[]{:S(2)}) copy-start(bf16[2048,4]{0,1:T(4,128)(2,1)} %param.18) | copy-start | bytes 49156
  91.9 6.8 %copy-start.2 = (bf16[2048,8]{0,1:T(8,128)(2,1)S(1)}, bf16[2048,8]{0,1:T(8,128)(2,1)}, u32[]{:S(2)}) copy-start(bf16[2048,8]{0,1:T(8,128)(2,1)} %param.19) | copy-start | bytes 98308
  93.7 41.7 %collective-permute-start = (bf16[8,256]{1,0:T(8,128)(2,1)S(1)}, bf16[8,256]{1,0:T(8,128)(2,1)S(1)}, u32[]{:S(2)}, u32[]{:S(2)}) collective-permute-start(bf16[8,256]{1,0:T(8,128)(2,1)S(1)} %get-tuple-element.6), channel_id=1, source_target_pairs={{0,4},{4,8},{8,12},{12,16},{16,20},{20,24},{24,28},{1,5},{5,9},{9,... | collective-permute-start | bytes 12296 | tf_op jit(solution)/shard_map/ppermute | solution.py:17
  97.0 38.3 %collective-permute-start.1 = (bf16[8,256]{1,0:T(8,128)(2,1)S(1)}, bf16[8,256]{1,0:T(8,128)(2,1)S(1)}, u32[]{:S(2)}, u32[]{:S(2)}) collective-permute-start(bf16[8,256]{1,0:T(8,128)(2,1)S(1)} %get-tuple-element.7), channel_id=1, source_target_pairs={{4,0},{8,4},{12,8},{16,12},{20,16},{24,20},{28,24},{5,1},{9,5},{13... | collective-permute-start | bytes 12296 | tf_op jit(solution)/shard_map/ppermute | solution.py:18
  129.8 25.6 %all-to-all-start.1 = ((bf16[8,96,512]{2,1,0:T(8,128)(2,1)}), bf16[8,96,512]{2,1,0:T(8,128)(2,1)S(1)}, u32[]{:S(2)}, u32[]{:S(2)}) async-start(bf16[8,96,512]{2,1,0:T(8,128)(2,1)} %reduce-scatter.2.cloned.1.call-done), calls=%async_computation.2 | async-start | bytes 1572864 | tf_op jit(solution)/shard_map/all_to_all | solution.py:129
Sparse Core Ops, SparseCore 0:
  49.4 27.5 all-gather.1
  92.1 37.7 reduce-scatter.1
where the time goes:
time: 167 us; the launch traced here: 166 us
  waiting for transfers between devices  71 us (43%)
  blocking collectives  33.3 us (20%)
  matrix products  16.8 us (10%)
  local copies, waits for them, and re-layouts  14.4 us (9%)
  between operations  14.4 us (9%)
  starting transfers between devices  10.2 us (6%)
  other arithmetic  6.05 us (4%)
    reduce_scatter x1, waiting for transfers between devices, routed_experts(): lax.psum_scatter(partial_out.reshape(sources, item_count, features).astyp...  30.7 us
    all_gather x1, waiting for transfers between devices, routed_experts(): arrived = lax.all_gather(arrived, 'tp', axis=2, tiled=True)  27.7 us
    all_to_all x1, blocking collectives, routed_experts(): lax.all_to_all(outgoing, 'ep', split_axis=0, concat_axis=0, tiled=True)  27.3 us
    all_to_all x1, waiting for transfers between devices, routed_experts(): lax.all_to_all(summed, 'ep', split_axis=0, concat_axis=0, tiled=True)  12.6 us
    dot_general x1, matrix products, routed_experts(): jnp.dot(flat_rows, expert_up[0], preferred_element_type=jnp.float32)  6.28 us
    all_gather x1, blocking collectives, token_mixer(): lax.all_gather(pooled, 'tp', axis=1, tiled=True)  5.96 us
    all_to_all x1, starting transfers between devices, routed_experts(): lax.all_to_all(summed, 'ep', split_axis=0, concat_axis=0, tiled=True)  5.51 us
    dot_general x1, matrix products, routed_experts(): jnp.dot(hidden, expert_down[0], preferred_element_type=jnp.float32)  4.81 us
  transfers between devices with their start and end apart: 5, of which 3 were waited for; matrix products, arithmetic and copies ran while one was open for 2% of the time, Pallas kernels for 0%

commit v1 on v0

v1 whole, which is shorter than its diff:
```python
import functools

import jax
import jax.numpy as jnp
from jax import lax
from jax.experimental import pallas as pl
from jax.experimental.pallas import tpu as pltpu
from jax.sharding import PartitionSpec as P

MESH = pl.DeviceIdType.MESH
EPSILON = 1e-06
HALO = 16
F32 = jnp.float32
BF16 = jnp.bfloat16


def tile_of(width, most):
    return most if width % most == 0 else width


def block_kernel(
    sizes,
    og_ref, pool_ref, ids_ref, weights_ref, wg_hbm, wu_hbm, wd_hbm, pw_hbm,
    mixed_ref, out_ref,
    wg, wu, wd, pw, rx, hid, part, core_in, y_in, answer, back, ext, pooled_all,
    w_sem, own_sem, d_send, d_recv, ay_send, ay_recv, ac_send, ac_recv,
    rc_send, rc_recv, ry_send, ry_recv, b_send, b_recv, h_send, h_recv, p_send, p_recv,
):
    E, T, steps, per_group = sizes
    Y = T // 2
    each = E // steps
    R, D = og_ref.shape[1], og_ref.shape[2]
    F, H = D // T, wg.shape[1]
    rows = each * R
    me, t = lax.axis_index("ep"), lax.axis_index("tp")
    y, c = t // 2, t % 2
    mate = t + 1 - 2 * c

    def ep_of(shift):
        return lax.rem(me + shift + E, E)

    def y_of(shift):
        return lax.rem(y + shift + Y, Y)

    def cols(index):
        return pl.ds(pl.multiple_of(index * F, F), F)

    def remote(src, dst, send, recv, where):
        return pltpu.make_async_remote_copy(
            src_ref=src, dst_ref=dst, send_sem=send, recv_sem=recv,
            device_id=where, device_id_type=MESH,
        )

    loads = [
        pltpu.make_async_copy(src, dst, w_sem.at[i])
        for i, (src, dst) in enumerate(((wg_hbm, wg), (wu_hbm, wu), (wd_hbm, wd), (pw_hbm, pw)))
    ]
    own = pltpu.make_async_copy(og_ref.at[me // per_group], rx.at[pl.ds(0, R)], own_sem)
    own.start()

    barrier = pltpu.get_barrier_semaphore()
    for d in range(1, E):
        pl.semaphore_signal(barrier, inc=1, device_id=(ep_of(d), t), device_id_type=MESH)
    for j in range(1, T):
        pl.semaphore_signal(
            barrier, inc=1, device_id=(me, lax.rem(t + j, T)), device_id_type=MESH
        )
    pl.semaphore_wait(barrier, E - 1 + T - 1)

    dispatch = {}
    for d in range(1, E):
        dest = ep_of(d)
        dispatch[d] = remote(
            og_ref.at[dest // per_group, :, cols(t)], rx.at[pl.ds(d * R, R), cols(t)],
            d_send.at[d], d_recv.at[d], (dest, t),
        )
        dispatch[d].start()
    n = pool_ref.shape[0]
    halo = [
        remote(pool_ref.at[pl.ds(n - HALO, HALO)], ext.at[pl.ds(0, HALO)],
               h_send.at[0], h_recv.at[0], (ep_of(1), t)),
        remote(pool_ref.at[pl.ds(0, HALO)], ext.at[pl.ds(n + HALO, HALO)],
               h_send.at[1], h_recv.at[1], (ep_of(-1), t)),
    ]
    for copy in halo:
        copy.start()
    for copy in loads:
        copy.start()

    gather_y, gather_c, give_c, give_y, answers = {}, {}, {}, {}, {}

    def span(g):
        first = g * rows + (R if g == 0 else 0)
        return pl.ds(first, (g + 1) * rows - first)

    def to_mate(g, j):
        place = rx.at[span(g), cols(2 * y_of(-j) + c)]
        gather_c[g, j] = remote(place, place, ac_send.at[g, j], ac_recv.at[g, j], (me, mate))
        gather_c[g, j].start()

    def arrive(g):
        for d in range(max(1, g * each), (g + 1) * each):
            dispatch[d].wait_recv()
        place = rx.at[span(g), cols(t)]
        for j in range(1, Y):
            gather_y[g, j] = remote(
                place, place, ay_send.at[g, j], ay_recv.at[g, j], (me, 2 * y_of(j) + c)
            )
            gather_y[g, j].start()
        to_mate(g, 0)

    def forward(g):
        for j in range(1, Y):
            gather_y[g, j].wait_recv()
            to_mate(g, j)

    def compute(g):
        for j in range(Y):
            gather_c[g, j].wait_recv()
        if g == 0:
            own.wait()
            loads[0].wait()
            loads[1].wait()
        block = pl.ds(g * rows, rows)
        width = tile_of(H, 256)

        @pl.loop(0, H // width)
        def _(i):
            at = pl.ds(pl.multiple_of(i * width, width), width)
            x = rx[block, :]
            gate = jnp.dot(x, wg[:, at], preferred_element_type=F32)
            up = jnp.dot(x, wu[:, at], preferred_element_type=F32)
            hid[:, at] = (gate / (1.0 + jnp.exp(-gate)) * up).astype(BF16)

        if g == 0:
            loads[2].wait()
        wide = tile_of(D, 512)

        @pl.loop(0, D // wide)
        def _(i):
            at = pl.ds(pl.multiple_of(i * wide, wide), wide)
            part[block, at] = jnp.dot(
                hid[...], wd[:, at], preferred_element_type=F32
            ).astype(BF16)

        for j in reversed(range(Y)):
            give_c[g, j] = remote(
                part.at[block, cols(2 * y_of(j) + 1 - c)], core_in.at[g, j],
                rc_send.at[g, j], rc_recv.at[g, j], (me, mate),
            )
            give_c[g, j].start()

    def reduce_core(g):
        block = pl.ds(g * rows, rows)
        for j in reversed(range(Y)):
            give_c[g, j].wait_recv()
            mine = part[block, cols(2 * y_of(j) + c)]
            core_in[g, j] = (core_in[g, j].astype(F32) + mine.astype(F32)).astype(BF16)
            if j:
                give_y[g, j] = remote(
                    core_in.at[g, j], y_in.at[g, j], ry_send.at[g, j], ry_recv.at[g, j],
                    (me, 2 * y_of(j) + c),
                )
                give_y[g, j].start()

    def reduce_y(g):
        total = core_in[g, 0].astype(F32)
        for j in range(1, Y):
            give_y[g, j].wait_recv()
            total += y_in[g, j].astype(F32)
        answer[pl.ds(g * rows, rows), :] = total.astype(BF16)
        for d in range(max(1, g * each), (g + 1) * each):
            answers[d] = remote(
                answer.at[pl.ds(d * R, R)], back.at[d], b_send.at[d], b_recv.at[d],
                (ep_of(-d), t),
            )
            answers[d].start()

    def pool():
        ext[pl.ds(HALO, n), :] = pool_ref[...]
        for copy in halo:
            copy.wait_recv()
        length = n * E
        channels = pool_ref.shape[1]
        half = jnp.left_shift(jnp.int32(1), t * channels // (channels * T // 4))
        at = me * n + lax.broadcasted_iota(jnp.int32, (n, n + 2 * HALO), 0)
        source = me * n - HALO + lax.broadcasted_iota(jnp.int32, (n, n + 2 * HALO), 1)
        low, high = jnp.maximum(at - half, 0), jnp.minimum(at + half, length)
        band = jnp.where((source >= low) & (source < high), 1.0, 0.0).astype(BF16)
        sums = jnp.dot(band, ext[...], preferred_element_type=F32)
        row = me * n + lax.broadcasted_iota(jnp.int32, (n, 1), 0)
        count = (jnp.minimum(row + half, length) - jnp.maximum(row - half, 0)).astype(F32)
        pooled_all[0] = (sums / count - pool_ref[...].astype(F32)).astype(BF16)
        sent = []
        for j in range(1, T):
            sent.append(remote(
                pooled_all.at[0], pooled_all.at[j], p_send.at[j], p_recv.at[j],
                (me, lax.rem(t + j, T)),
            ))
            sent[-1].start()
        return sent

    def mix(sent):
        loads[3].wait()
        total = jnp.dot(pooled_all[0], pw[t], preferred_element_type=F32)
        for j in range(1, T):
            sent[j - 1].wait_recv()
            total += jnp.dot(
                pooled_all[j], pw[lax.rem(t + T - j, T)], preferred_element_type=F32
            )
        mixed_ref[...] = total.astype(BF16)

    sent = pool()
    stages = (arrive, forward, compute, reduce_core, reduce_y)
    lead = (0, 1, 2, 3, 4)
    for beat in range(steps + lead[-1]):
        for stage, late in zip(stages, lead):
            if 0 <= beat - late < steps:
                stage(beat - late)
        if beat == 1:
            mix(sent)

    slot = ids_ref[:, 0:1]
    first, second = ids_ref[:, 1:2], ids_ref[:, 2:3]
    first_weight, second_weight = weights_ref[:, 0:1], weights_ref[:, 1:2]
    local = ids_ref.shape[0]
    place = lax.broadcasted_iota(jnp.int32, (local, R), 1)
    total = jnp.zeros((local, F), F32)
    for d in range(E):
        expert = ep_of(d)
        weight = jnp.where(first == expert, first_weight, jnp.where(second == expert, second_weight, 0.0))
        pick = jnp.where(slot == place + expert // per_group * R, weight, 0.0)
        high = pick.astype(BF16)
        low = (pick - high.astype(F32)).astype(BF16)
        if d == 0:
            rows_back = answer[pl.ds(0, R), :]
        else:
            answers[d].wait_recv()
            rows_back = back[d]
        total += jnp.dot(high, rows_back, preferred_element_type=F32)
        total += jnp.dot(low, rows_back, preferred_element_type=F32)
    out_ref[...] = total.astype(BF16)

    for group in (dispatch, gather_y, gather_c, give_c, give_y, answers):
        for copy in group.values():
            copy.wait_send()
    for copy in halo + sent:
        copy.wait_send()


def normalize(row_data, gain_vector):
    values = row_data.astype(F32)
    inverse_rms = lax.rsqrt(jnp.mean(values * values, axis=-1, keepdims=True) + EPSILON)
    return (values * inverse_rms * gain_vector).astype(BF16)


def on_device(
    mix_input, mix_gain, pool_in_weight, pool_out_weight, moe_input, moe_gain,
    group_router, expert_router, routes, expert_gate, expert_up, expert_down,
):
    E, T = lax.axis_size("ep"), lax.axis_size("tp")
    normed_moe = normalize(moe_input, moe_gain)
    local, D = normed_moe.shape
    groups, experts = group_router.shape[1], expert_router.shape[1]
    per_group = experts // groups
    R = 2 * local // groups
    chosen = routes[:, 0] // per_group
    match = jnp.arange(groups, dtype=jnp.int32)[None, :] == chosen[:, None]
    places = jnp.arange(local, dtype=jnp.int32)
    before = (places[None, :] < places[:, None]) & (chosen[None, :] == chosen[:, None])
    rank = jnp.sum(before.astype(jnp.int32), axis=1)
    slot = chosen * R + rank
    select = (jnp.arange(groups * R, dtype=jnp.int32)[:, None] == slot[None, :]).astype(BF16)
    outgoing = jnp.dot(select, normed_moe, preferred_element_type=F32).astype(BF16)
    outgoing = outgoing.reshape(groups, R, D)

    logits = jnp.dot(
        normed_moe, jnp.concatenate([group_router, expert_router], axis=1),
        preferred_element_type=F32,
    )
    group_logits, expert_logits = logits[:, :groups], logits[:, groups:]
    chosen_logit = jnp.sum(jnp.where(match, group_logits, 0.0), axis=1)
    share = 1.0 / jnp.sum(jnp.exp(group_logits - chosen_logit[:, None]), axis=1)
    expert_ids = jnp.arange(experts, dtype=jnp.int32)[None, :]
    first_logit = jnp.sum(jnp.where(expert_ids == routes[:, 0:1], expert_logits, 0.0), axis=1)
    second_logit = jnp.sum(jnp.where(expert_ids == routes[:, 1:2], expert_logits, 0.0), axis=1)
    weights = jnp.stack(
        [share * jax.nn.sigmoid(first_logit - second_logit),
         share * jax.nn.sigmoid(second_logit - first_logit)], axis=1)
    ids = jnp.concatenate([slot[:, None], routes], axis=1)

    pool_input = jnp.dot(
        normalize(mix_input, mix_gain), pool_in_weight, preferred_element_type=F32
    ).astype(BF16)

    n, channels = pool_input.shape
    F, H, Y = D // T, expert_gate.shape[2], T // 2
    F2 = pool_out_weight.shape[1]
    steps = 4
    rows = E // steps * R
    dma = pltpu.SemaphoreType.DMA
    vmem = pl.BlockSpec(memory_space=pltpu.VMEM)
    hbm = pl.BlockSpec(memory_space=pl.ANY)
    return pl.pallas_call(
        functools.partial(block_kernel, (E, T, steps, per_group)),
        out_shape=(
            jax.ShapeDtypeStruct((n, F2), BF16),
            jax.ShapeDtypeStruct((local, F), BF16),
        ),
        in_specs=[vmem] * 4 + [hbm] * 4,
        out_specs=(vmem, vmem),
        scratch_shapes=[
            pltpu.VMEM((D, H), BF16),
            pltpu.VMEM((D, H), BF16),
            pltpu.VMEM((H, D), BF16),
            pltpu.VMEM((T, channels, F2), BF16),
            pltpu.VMEM((E * R, D), BF16),
            pltpu.VMEM((rows, H), BF16),
            pltpu.VMEM((E * R, D), BF16),
            pltpu.VMEM((steps, Y, rows, F), BF16),
            pltpu.VMEM((steps, Y, rows, F), BF16),
            pltpu.VMEM((E * R, F), BF16),
            pltpu.VMEM((E, R, F), BF16),
            pltpu.VMEM((n + 2 * HALO, channels), BF16),
            pltpu.VMEM((T, n, channels), BF16),
            dma((4,)), dma, dma((E,)), dma((E,)),
            dma((steps, Y)), dma((steps, Y)), dma((steps, Y)), dma((steps, Y)),
            dma((steps, Y)), dma((steps, Y)), dma((steps, Y)), dma((steps, Y)),
            dma((E,)), dma((E,)), dma((2,)), dma((2,)), dma((T,)), dma((T,)),
        ],
        compiler_params=pltpu.CompilerParams(
            collective_id=0, has_side_effects=True, vmem_limit_bytes=60 * 1024 * 1024
        ),
    )(
        outgoing, pool_input, ids, weights,
        expert_gate.reshape(D, H), expert_up.reshape(D, H), expert_down.reshape(H, D),
        pool_out_weight.reshape(T, channels, F2),
    )


def solution(mesh):
    in_specs = (
        P("ep", None), P(), P(None, "tp"), P(None, "tp"), P("ep", None), P(), P(), P(),
        P("ep", None), P("ep", None, "tp"), P("ep", None, "tp"), P("ep", "tp", None),
    )
    return jax.shard_map(
        on_device, mesh=mesh, in_specs=in_specs, out_specs=(P("ep", "tp"), P("ep", "tp")),
        check_vma=False,
    )
```

time: 167 us -> 88.9 us (0.53)
  Pallas kernels: 0 us -> 74.1 us
  waiting for transfers between devices: 71 us -> 0 us
  blocking collectives: 33.3 us -> 0 us
  between operations: 14.4 us -> 0.74 us
  matrix products: 16.8 us -> 4.43 us
  starting transfers between devices: 10.2 us -> 0 us
  local copies, waits for them, and re-layouts: 14.4 us -> 4.75 us
    pallas_call x0 -> x1, Pallas kernels: none -> 74.1 us  [on_device(): pl.pallas_call(functools.partial(block_kernel, (E, T, steps, per_group)),...]
    reduce_scatter x1 -> x0, waiting for transfers between devices: 30.7 us -> none  [routed_experts(): lax.psum_scatter(partial_out.reshape(sources, item_count, features).astyp...]
    all_gather x1 -> x0, waiting for transfers between devices: 27.7 us -> none  [routed_experts(): arrived = lax.all_gather(arrived, 'tp', axis=2, tiled=True)]
    all_to_all x1 -> x0, blocking collectives: 27.3 us -> none  [routed_experts(): lax.all_to_all(outgoing, 'ep', split_axis=0, concat_axis=0, tiled=True)]
    all_to_all x1 -> x0, waiting for transfers between devices: 12.6 us -> none  [routed_experts(): lax.all_to_all(summed, 'ep', split_axis=0, concat_axis=0, tiled=True)]
    dot_general x7 -> x3, matrix products: 16.8 us -> 4.43 us  [the longest x1 1.85 us: on_device(): jnp.dot(select, normed_moe, preferred_element_type=F32).astype(BF16)]
    gather x2 -> x0, local copies, waits for them, and re-layouts: 6.33 us -> none  [the longest x1 4.27 us: routed_experts(): outgoing = padded[slot_copy // 2].reshape(expert_count, capacity, features)]
    all_gather x1 -> x0, blocking collectives: 5.96 us -> none  [token_mixer(): lax.all_gather(pooled, 'tp', axis=1, tiled=True)]
  transfers between devices with their start and end apart: 5 -> 0, of which waited for: 3 -> 0; matrix products, arithmetic and copies ran while one was open for 2% -> 0% of each run, Pallas kernels for 0% -> 0%
where the time goes in v1:
time: 88.9 us; the launch traced here: 88.6 us
  Pallas kernels  74.1 us (83%)
  local copies, waits for them, and re-layouts  4.75 us (5%)
  other arithmetic  4.51 us (5%)
  matrix products  4.43 us (5%)
    pallas_call x1, Pallas kernels, on_device(): pl.pallas_call(functools.partial(block_kernel, (E, T, steps, per_group)),...  74.1 us
    unnamed x12, local copies, waits for them, and re-layouts  3.21 us
    reduce_sum x2, other arithmetic, normalize(): jnp.mean(values * values, axis=-1, keepdims=True) + EPSILON  2.72 us
    dot_general x1, matrix products, on_device(): jnp.dot(select, normed_moe, preferred_element_type=F32).astype(BF16)  1.85 us

profile of v1, /device:TPU:0, one launch (start us, length us, event | category | flops | bytes accessed | tf_op | source)
XLA Modules:
  0.0 88.6 jit_solution(2946251413814136381)
XLA Ops:
  0.6 0.0 copy-start
  0.6 0.0 copy-start.2
  0.7 0.0 copy-start.4
  0.7 1.3 %fusion.3 = f32[128]{0:T(128)S(1)} fusion(bf16[128,2048]{1,0:T(8,128)(2,1)} %param.12), kind=kLoop, calls=%fused_computation.9 | loop fusion | flops 786304 | bytes 524800 | tf_op jit(solution)/shard_map/reduce_sum | solution.py:253
  2.0 1.4 %fusion = f32[192]{0:T(256)S(1)} fusion(bf16[192,2048]{1,0:T(8,128)(2,1)} %param.16), kind=kLoop, calls=%fused_computation.3 | loop fusion | flops 1179456 | bytes 787200 | tf_op jit(solution)/shard_map/reduce_sum | solution.py:253
  3.4 0.8 fusion.18
  4.2 0.2 convert_reduce_fusion
  4.4 0.7 pad_add_fusion
  5.1 0.0 copy-start.1
  5.1 0.0 copy-start.3
  5.1 1.6 %fusion.9 = f32[192,12]{0,1:T(8,128)S(1)} fusion(bf16[192,2048]{1,0:T(8,128)(2,1)} %param.16, f32[2048]{0:T(1024)} %param.17, f32[192]{0:T(256)S(1)} %add_rsqrt_fusion, bf16[2048,8]{0,1:T(8,128)(2,1)} %param.19, bf16[2048,4]{0,1:T(4,128)(2,1)} %param.18), kind=kOutput, calls=%fused_computation.15 | convolution fusion | flops 11108352 | bytes 853760 | tf_op jit(solution)/shard_map/dot_general | solution.py:277
  6.8 0.0 copy-done
  6.9 0.0 copy-done.2
  6.9 0.0 copy-done.4
  6.9 1.0 %convolution_convert_fusion.1.pool_ref = bf16[128,256]{1,0:T(8,128)(2,1)} fusion(bf16[2048,256]{1,0:T(8,128)(2,1)S(1)} %copy-done, bf16[128,2048]{1,0:T(8,128)(2,1)S(1)} %copy-done.2, f32[2048]{0:T(1024)S(1)} %copy-done.4, f32[128]{0:T(128)S(1)} %add_rsqrt_fusion.1), kind=kOutput, calls=%fused_computation.8 | convolution fusion | flops 135299072 | bytes 1647104 | tf_op jit(solution)/shard_map/dot_general | solution.py:292
  7.8 0.8 copy.23.ids_ref
  8.6 0.8 copy.24.weights_ref
  9.4 0.0 copy-done.1
  9.4 0.0 copy-done.3
  9.4 1.9 %convolution_convert_fusion = bf16[384,2048]{1,0:T(8,128)(2,1)} fusion(bf16[192,2048]{1,0:T(8,128)(2,1)S(1)} %copy-done.1, f32[2048]{0:T(1024)S(1)} %copy-done.3, f32[192]{0:T(256)S(1)} %add_rsqrt_fusion, s32[192]{0:T(256)S(1)} %multiply_add_fusion.1), kind=kOutput, calls=%fused_computation | convolution fusion | flops 304422912 | bytes 2369024 | tf_op jit(solution)/shard_map/dot_general | solution.py:274
  11.2 74.1 %shard_map.131 = (bf16[128,512]{1,0:T(8,128)(2,1)}, bf16[192,512]{1,0:T(8,128)(2,1)}) custom-call(bf16[4,96,2048]{2,1,0:T(8,128)(2,1)} %bitcast.12, bf16[128,256]{1,0:T(8,128)(2,1)} %convolution_convert_fusion.1.pool_ref, s32[192,3]{1,0:T(8,128)} %copy.23.ids_ref, f32[192,2]{1,0:T(8,128)} %copy.24.weights_ref, bf16[2048,1024]{1,0:T(8,128)(2,1)} %bitcast.13, ...), custom_call_target="tpu_custom_call" | custom-call | tf_op jit(solution)/shard_map/pallas_call | solution.py:304
  85.4 1.6 %copy.27 = bf16[128,512]{1,0:T(8,128)(2,1)} copy(bf16[128,512]{1,0:T(8,128)(2,1)} %get-tuple-element.11) | data formatting | bytes 262144
  86.9 1.6 %copy.28 = bf16[192,512]{1,0:T(8,128)(2,1)} copy(bf16[192,512]{1,0:T(8,128)(2,1)} %get-tuple-element.12) | data formatting | bytes 393216
  (10 shorter events, 0.1 us)
Async XLA Ops:
  0.6 6.2 %copy-start = (bf16[2048,256]{1,0:T(8,128)(2,1)S(1)}, bf16[2048,256]{1,0:T(8,128)(2,1)}, u32[]{:S(2)}) copy-start(bf16[2048,256]{1,0:T(8,128)(2,1)} %param.14) | copy-start | bytes 3145732
  0.6 6.2 %copy-start.2 = (bf16[128,2048]{1,0:T(8,128)(2,1)S(1)}, bf16[128,2048]{1,0:T(8,128)(2,1)}, u32[]{:S(2)}) copy-start(bf16[128,2048]{1,0:T(8,128)(2,1)} %param.12) | copy-start | bytes 1572868
  0.7 6.2 %copy-start.4 = (f32[2048]{0:T(1024)S(1)}, f32[2048]{0:T(1024)}, u32[]{:S(2)}) copy-start(f32[2048]{0:T(1024)} %param.13) | copy-start | bytes 24580
  5.1 4.3 %copy-start.1 = (bf16[192,2048]{1,0:T(8,128)(2,1)S(1)}, bf16[192,2048]{1,0:T(8,128)(2,1)}, u32[]{:S(2)}) copy-start(bf16[192,2048]{1,0:T(8,128)(2,1)} %param.16) | copy-start | bytes 2359300
  5.1 4.3 %copy-start.3 = (f32[2048]{0:T(1024)S(1)}, f32[2048]{0:T(1024)}, u32[]{:S(2)}) copy-start(f32[2048]{0:T(1024)} %param.17) | copy-start | bytes 24580

commit v2 on v1

--- a/solution.py
+++ b/solution.py
@@ -18,18 +18,31 @@
     return most if width % most == 0 else width
 
 
+def normalize(rows_ref, gain_ref, result):
+    count = 32 if rows_ref.shape[0] % 32 == 0 else rows_ref.shape[0]
+
+    @pl.loop(0, rows_ref.shape[0] // count)
+    def _(i):
+        at = pl.ds(pl.multiple_of(i * count, count), count)
+        values = rows_ref[at, :].astype(F32)
+        inverse_rms = lax.rsqrt(jnp.mean(values * values, axis=-1, keepdims=True) + EPSILON)
+        result[at, :] = (values * inverse_rms * gain_ref[...]).astype(BF16)
+
+
 def block_kernel(
     sizes,
-    og_ref, pool_ref, ids_ref, weights_ref, wg_hbm, wu_hbm, wd_hbm, pw_hbm,
+    mix_ref, mix_gain_ref, pool_in_ref, moe_ref, moe_gain_ref, router_ref, routes_ref, wg_hbm, wu_hbm, wd_hbm, pw_hbm,
     mixed_ref, out_ref,
-    wg, wu, wd, pw, rx, hid, part, core_in, y_in, answer, back, ext, pooled_all,
+    og, normed, normed_mix, pool_ref, wg, wu, wd, pw, rx, hid, part, core_in, y_in, answer, back, ext, pooled_all,
     w_sem, own_sem, d_send, d_recv, ay_send, ay_recv, ac_send, ac_recv,
     rc_send, rc_recv, ry_send, ry_recv, b_send, b_recv, h_send, h_recv, p_send, p_recv,
 ):
     E, T, steps, per_group = sizes
     Y = T // 2
     each = E // steps
-    R, D = og_ref.shape[1], og_ref.shape[2]
+    local, D = moe_ref.shape
+    groups = E // per_group
+    R = 2 * local // groups
     F, H = D // T, wg.shape[1]
     rows = each * R
     me, t = lax.axis_index("ep"), lax.axis_index("tp")
@@ -55,8 +68,8 @@
         pltpu.make_async_copy(src, dst, w_sem.at[i])
         for i, (src, dst) in enumerate(((wg_hbm, wg), (wu_hbm, wu), (wd_hbm, wd), (pw_hbm, pw)))
     ]
-    own = pltpu.make_async_copy(og_ref.at[me // per_group], rx.at[pl.ds(0, R)], own_sem)
-    own.start()
+    for copy in loads:
+        copy.start()
 
     barrier = pltpu.get_barrier_semaphore()
     for d in range(1, E):
@@ -65,16 +78,44 @@
         pl.semaphore_signal(
             barrier, inc=1, device_id=(me, lax.rem(t + j, T)), device_id_type=MESH
         )
+
+    normalize(mix_ref, mix_gain_ref, normed_mix)
+    pool_ref[...] = jnp.dot(normed_mix[...], pool_in_ref[...], preferred_element_type=F32).astype(BF16)
+    normalize(moe_ref, moe_gain_ref, normed)
+    first, second = routes_ref[:, 0:1], routes_ref[:, 1:2]
+
+    def lanes(width):
+        return lax.broadcasted_iota(jnp.int32, (local, width), 1)
+
+    lane = lanes(128)
+    low = lane * per_group
+    match = (first >= low) & (first < low + per_group) & (lane < groups)
+    before = lax.broadcasted_iota(jnp.int32, (local, local), 0) > lanes(local)
+    rank = jnp.dot(
+        jnp.where(before, 1.0, 0.0).astype(BF16), jnp.where(match, 1.0, 0.0).astype(BF16),
+        preferred_element_type=F32,
+    )
+    slot = jnp.sum(
+        jnp.where(match, rank + (lane * R).astype(F32), 0.0), axis=1, keepdims=True
+    ).astype(jnp.int32)
+    select = jnp.where(lanes(groups * R) == slot, 1.0, 0.0).astype(BF16)
+    piece = tile_of(D, 512)
+
+    @pl.loop(0, D // piece)
+    def _(i):
+        at = pl.ds(pl.multiple_of(i * piece, piece), piece)
+        og[:, at] = lax.dot_general(
+            select, normed[:, at], (((0,), (0,)), ((), ())), preferred_element_type=F32
+        ).astype(BF16)
+
     pl.semaphore_wait(barrier, E - 1 + T - 1)
 
-    dispatch = {}
-    for d in range(1, E):
-        dest = ep_of(d)
-        dispatch[d] = remote(
-            og_ref.at[dest // per_group, :, cols(t)], rx.at[pl.ds(d * R, R), cols(t)],
-            d_send.at[d], d_recv.at[d], (dest, t),
-        )
-        dispatch[d].start()
+    def group_rows(expert):
+        return pl.ds(pl.multiple_of(expert // per_group * R, R), R)
+
+    own = pltpu.make_async_copy(og.at[group_rows(me)], rx.at[pl.ds(0, R)], own_sem)
+    own.start()
+
     n = pool_ref.shape[0]
     halo = [
         remote(pool_ref.at[pl.ds(n - HALO, HALO)], ext.at[pl.ds(0, HALO)],
@@ -84,8 +125,15 @@
     ]
     for copy in halo:
         copy.start()
-    for copy in loads:
-        copy.start()
+    dispatch = {}
+    for d in range(1, E):
+        dest = ep_of(d)
+        part_of = cols(t)
+        dispatch[d] = remote(
+            og.at[group_rows(dest), part_of], rx.at[pl.ds(d * R, R), part_of],
+            d_send.at[d], d_recv.at[d], (dest, t),
+        )
+        dispatch[d].start()
 
     gather_y, gather_c, give_c, give_y, answers = {}, {}, {}, {}, {}
 
@@ -210,6 +258,20 @@
             )
         mixed_ref[...] = total.astype(BF16)
 
+    logits = jnp.dot(normed[...], router_ref[...], preferred_element_type=F32)
+    lane = lanes(groups + E)
+    low = lane * per_group
+    match = (first >= low) & (first < low + per_group) & (lane < groups)
+
+    def logit_at(mask):
+        return jnp.sum(jnp.where(mask, logits, 0.0), axis=1, keepdims=True)
+
+    spread = jnp.where(lane < groups, jnp.exp(logits - logit_at(match)), 0.0)
+    share = 1.0 / jnp.sum(spread, axis=1, keepdims=True)
+    gap = logit_at(lane == first + groups) - logit_at(lane == second + groups)
+    first_weight = share / (1.0 + jnp.exp(-gap))
+    second_weight = share / (1.0 + jnp.exp(gap))
+
     sent = pool()
     stages = (arrive, forward, compute, reduce_core, reduce_y)
     lead = (0, 1, 2, 3, 4)
@@ -217,14 +279,10 @@
         for stage, late in zip(stages, lead):
             if 0 <= beat - late < steps:
                 stage(beat - late)
-        if beat == 1:
+        if beat == steps + 1:
             mix(sent)
 
-    slot = ids_ref[:, 0:1]
-    first, second = ids_ref[:, 1:2], ids_ref[:, 2:3]
-    first_weight, second_weight = weights_ref[:, 0:1], weights_ref[:, 1:2]
-    local = ids_ref.shape[0]
-    place = lax.broadcasted_iota(jnp.int32, (local, R), 1)
+    place = lanes(R)
     total = jnp.zeros((local, F), F32)
     for d in range(E):
         expert = ep_of(d)
@@ -248,52 +306,16 @@
         copy.wait_send()
 
 
-def normalize(row_data, gain_vector):
-    values = row_data.astype(F32)
-    inverse_rms = lax.rsqrt(jnp.mean(values * values, axis=-1, keepdims=True) + EPSILON)
-    return (values * inverse_rms * gain_vector).astype(BF16)
-
-
 def on_device(
     mix_input, mix_gain, pool_in_weight, pool_out_weight, moe_input, moe_gain,
     group_router, expert_router, routes, expert_gate, expert_up, expert_down,
 ):
     E, T = lax.axis_size("ep"), lax.axis_size("tp")
-    normed_moe = normalize(moe_input, moe_gain)
-    local, D = normed_moe.shape
+    local, D = moe_input.shape
     groups, experts = group_router.shape[1], expert_router.shape[1]
     per_group = experts // groups
     R = 2 * local // groups
-    chosen = routes[:, 0] // per_group
-    match = jnp.arange(groups, dtype=jnp.int32)[None, :] == chosen[:, None]
-    places = jnp.arange(local, dtype=jnp.int32)
-    before = (places[None, :] < places[:, None]) & (chosen[None, :] == chosen[:, None])
-    rank = jnp.sum(before.astype(jnp.int32), axis=1)
-    slot = chosen * R + rank
-    select = (jnp.arange(groups * R, dtype=jnp.int32)[:, None] == slot[None, :]).astype(BF16)
-    outgoing = jnp.dot(select, normed_moe, preferred_element_type=F32).astype(BF16)
-    outgoing = outgoing.reshape(groups, R, D)
-
-    logits = jnp.dot(
-        normed_moe, jnp.concatenate([group_router, expert_router], axis=1),
-        preferred_element_type=F32,
-    )
-    group_logits, expert_logits = logits[:, :groups], logits[:, groups:]
-    chosen_logit = jnp.sum(jnp.where(match, group_logits, 0.0), axis=1)
-    share = 1.0 / jnp.sum(jnp.exp(group_logits - chosen_logit[:, None]), axis=1)
-    expert_ids = jnp.arange(experts, dtype=jnp.int32)[None, :]
-    first_logit = jnp.sum(jnp.where(expert_ids == routes[:, 0:1], expert_logits, 0.0), axis=1)
-    second_logit = jnp.sum(jnp.where(expert_ids == routes[:, 1:2], expert_logits, 0.0), axis=1)
-    weights = jnp.stack(
-        [share * jax.nn.sigmoid(first_logit - second_logit),
-         share * jax.nn.sigmoid(second_logit - first_logit)], axis=1)
-    ids = jnp.concatenate([slot[:, None], routes], axis=1)
-
-    pool_input = jnp.dot(
-        normalize(mix_input, mix_gain), pool_in_weight, preferred_element_type=F32
-    ).astype(BF16)
-
-    n, channels = pool_input.shape
+    n, channels = mix_input.shape[0], pool_in_weight.shape[1]
     F, H, Y = D // T, expert_gate.shape[2], T // 2
     F2 = pool_out_weight.shape[1]
     steps = 4
@@ -307,9 +329,13 @@
             jax.ShapeDtypeStruct((n, F2), BF16),
             jax.ShapeDtypeStruct((local, F), BF16),
         ),
-        in_specs=[vmem] * 4 + [hbm] * 4,
+        in_specs=[vmem] * 7 + [hbm] * 4,
         out_specs=(vmem, vmem),
         scratch_shapes=[
+            pltpu.VMEM((groups * R, D), BF16),
+            pltpu.VMEM((local, D), BF16),
+            pltpu.VMEM((n, D), BF16),
+            pltpu.VMEM((n, channels), BF16),
             pltpu.VMEM((D, H), BF16),
             pltpu.VMEM((D, H), BF16),
             pltpu.VMEM((H, D), BF16),
@@ -332,7 +358,8 @@
             collective_id=0, has_side_effects=True, vmem_limit_bytes=60 * 1024 * 1024
         ),
     )(
-        outgoing, pool_input, ids, weights,
+        mix_input, mix_gain[None, :], pool_in_weight, moe_input, moe_gain[None, :],
+        jnp.concatenate([group_router, expert_router], axis=1), routes,
         expert_gate.reshape(D, H), expert_up.reshape(D, H), expert_down.reshape(H, D),
         pool_out_weight.reshape(T, channels, F2),
     )

time: 88.9 us -> 76 us (0.85)
  Pallas kernels: 74.1 us -> 68.7 us
  matrix products: 4.43 us -> 0 us
  other arithmetic: 4.51 us -> 0.78 us
  local copies, waits for them, and re-layouts: 4.75 us -> 5.66 us
    pallas_call x1, Pallas kernels: 74.1 us -> 68.7 us  [on_device(): pl.pallas_call(functools.partial(block_kernel, (E, T, steps, per_group)),...]
    dot_general x3 -> x0, matrix products: 4.43 us -> none  [the longest x1 1.85 us: on_device(): jnp.dot(select, normed_moe, preferred_element_type=F32).astype(BF16)]
    reduce_sum x6 -> x0, other arithmetic: 2.98 us -> none  [the longest x2 2.72 us: normalize(): jnp.mean(values * values, axis=-1, keepdims=True) + EPSILON]
    unnamed x12 -> x3, local copies, waits for them, and re-layouts: 3.21 us -> 4.63 us
where the time goes in v2:
time: 76 us; the launch traced here: 75.7 us
  Pallas kernels  68.7 us (90%)
  local copies, waits for them, and re-layouts  5.66 us (7%)
  other arithmetic  0.78 us (1%)
    pallas_call x1, Pallas kernels, on_device(): pl.pallas_call(functools.partial(block_kernel, (E, T, steps, per_group)),...  68.7 us
    unnamed x3, local copies, waits for them, and re-layouts  4.63 us

profile of v2, /device:TPU:0, one launch (start us, length us, event | category | flops | bytes accessed | tf_op | source)
XLA Modules:
  0.0 75.7 jit_solution(9747015402755324176)
XLA Ops:
  0.6 0.8 %pad_maximum_fusion = bf16[2048,12]{0,1:T(8,128)(2,1)S(1)} fusion(bf16[2048,8]{0,1:T(8,128)(2,1)} %param.19, bf16[2048,4]{0,1:T(4,128)(2,1)} %param.18), kind=kLoop, calls=%fused_computation | loop fusion | flops 98304 | bytes 98304 | tf_op jit(solution)/shard_map/concatenate | solution.py:362
  1.4 1.4 %copy.18.routes_ref = s32[192,2]{1,0:T(8,128)} copy(s32[192,2]{0,1:T(2,128)} %param.20) | data formatting | bytes 3072 | tf_op args[8]
  2.9 1.0 %copy.17.router_ref = bf16[2048,12]{1,0:T(8,128)(2,1)} copy(bf16[2048,12]{0,1:T(8,128)(2,1)S(1)} %pad_maximum_fusion) | data formatting | bytes 98304 | tf_op jit(solution)/shard_map/concatenate | solution.py:362
  3.9 68.7 %shard_map.131 = (bf16[128,512]{1,0:T(8,128)(2,1)}, bf16[192,512]{1,0:T(8,128)(2,1)}) custom-call(bf16[128,2048]{1,0:T(8,128)(2,1)} %mix_ref.1, f32[1,2048]{1,0:T(1,128)} %bitcast.10, bf16[2048,256]{1,0:T(8,128)(2,1)} %pool_in_ref.1, bf16[192,2048]{1,0:T(8,128)(2,1)} %moe_ref.1, f32[1,2048]{1,0:T(1,128)} %bitcast.11, bf16[2048,12]{1,0:T(8,128)(2,1)} %copy.17.router_ref, ...), custom_call_target="tpu_custom_call" | custom-call | tf_op jit(solution)/shard_map/pallas_call | solution.py:326
  72.6 1.6 %copy.21 = bf16[128,512]{1,0:T(8,128)(2,1)} copy(bf16[128,512]{1,0:T(8,128)(2,1)} %get-tuple-element.4) | data formatting | bytes 262144
  74.1 1.6 %copy.22 = bf16[192,512]{1,0:T(8,128)(2,1)} copy(bf16[192,512]{1,0:T(8,128)(2,1)} %get-tuple-element.5) | data formatting | bytes 393216
